TPU v7x, 512 devices: a 4x2x32 block of a 4x8x32 slice. The times are simulated.
512 devices in a mesh: grp: 2 (over y), fs: 32 (over z), tp: 8 (over x, core).
Axes of the slice: x: 4, y: 2, z: 32, core: 2. Of those that a mesh axis runs over, the one named last changes fastest.
The devices are a block of a 4x8x32 slice.
Arguments:
- tokens: bfloat16 [16384, 2048], P(('grp', 'fs'), 'tp'), parts along dimension 0, may hold values from -6 to 6
- recurrent_norm_gain: float32 [2048], replicated, may hold values from 0.1 to 1.9
- feedforward_norm_gain: float32 [2048], replicated, may hold values from 0.1 to 1.9
- gate_projection_weight: bfloat16 [2048, 2048], P('fs', 'tp'), may hold values from -0.125 to 0.125
- recurrent_projection_weight: bfloat16 [2048, 2048], P('fs', 'tp'), may hold values from -0.125 to 0.125
- convolution_kernel: bfloat16 [4, 2048], P(None, 'tp'), may hold values from -3 to 3
- decay_gate_matrix: bfloat16 [16, 128, 128], P('tp'), may hold values from -0.5 to 0.5
- input_gate_matrix: bfloat16 [16, 128, 128], P('tp'), may hold values from -0.5 to 0.5
- base_decay_logit: float32 [2048], P('tp'), may hold values from 3 to 9
- extra_log_decay: float32 [16384], P(('grp', 'fs')), parts along dimension 0, may hold values from -0.7 to 0
- output_projection_weight: bfloat16 [2048, 2048], P('tp', 'fs'), may hold values from -0.125 to 0.125
- up_projection_weight: bfloat16 [2048, 8192], P('fs', 'tp'), may hold values from -0.125 to 0.125
- down_projection_weight: bfloat16 [8192, 2048], P('tp', 'fs'), may hold values from -0.0625 to 0.0625
Outputs:
- layer_out: bfloat16 [16384, 2048], P(('grp', 'fs'), 'tp'), parts along dimension 0
There are 2 independent parts, one for each index of `grp`. A program takes and returns all parts, laid end to end along the dimension named above; an argument that names none is the same for every part. Nothing has to cross between parts.
All inputs are finite; a program needn't handle non-finite values.
Results may differ from a plain program's by a relative error of at most 0.018.
Values may be sent and summed in bfloat16 or wider, within the bound.
No kernel may reach another device: no remote copies, remote signals or barrier semaphores. Data moves between devices by JAX's collectives and lax.ppermute only.
A program may use at most 64 MiB of HBM per device.

v0:
```python
import jax
import jax.numpy as jnp
from jax import lax
from jax.sharding import PartitionSpec as P


def from_everyone(x, axis):
    copies = jnp.broadcast_to(x, (lax.axis_size(axis), *x.shape))
    return lax.all_to_all(copies, axis, split_axis=0, concat_axis=0, tiled=True)


def laid_out(tiles, dim):
    tiles = jnp.moveaxis(tiles, 0, dim)
    lengths = tiles.shape
    return tiles.reshape(*lengths[:dim], lengths[dim] * lengths[dim + 1], *lengths[dim + 2 :])


def collect(x, axis, dim):
    tiles = from_everyone(x, axis)
    return laid_out(tiles, dim)


def gather_turned(arrays, axis, dims):
    turned = [jnp.moveaxis(a, dim, 0) for a, dim in zip(arrays, dims)]
    widths = [t[0].size for t in turned]
    both = jnp.concatenate([t.reshape(-1, w) for t, w in zip(turned, widths)], axis=1)
    out = lax.all_gather(both, axis, axis=0, tiled=True)
    tiles = jnp.split(out, [sum(widths[:k]) for k in range(1, len(widths))], axis=1)
    return tuple(
        (
            jnp.moveaxis(b.reshape(-1, *t.shape[1:]), 0, dim)
            for b, t, dim in zip(tiles, turned, dims)
        )
    )


def in_blocks(x, dim, peers):
    lengths = x.shape
    tiles = x.reshape(*lengths[:dim], peers, lengths[dim] // peers, *lengths[dim + 1 :])
    return jnp.moveaxis(tiles, dim, 0)


def sent_and_summed(x, axis, dim):
    peers = lax.axis_size(axis)
    tiles = lax.all_to_all(in_blocks(x, dim, peers), axis, 0, 0, tiled=True)
    return jnp.sum(tiles.astype(jnp.float32), axis=0)


def rms_rows(values_in, norm_gain):
    values = values_in.astype(jnp.float32)
    inverse = lax.rsqrt(jnp.mean(values * values, axis=-1, keepdims=True) + 1e-06)
    return (values * inverse * norm_gain).astype(jnp.bfloat16)


def combine(earlier, later):
    return (earlier[0] * later[0], later[0] * earlier[1] + later[1])


def recurrent_state(
    recurrent_branch_rows,
    gate_branch_rows,
    convolution_kernel,
    decay_gate_matrix,
    input_gate_matrix,
    base_decay_logit,
    extra_log_decay,
):
    length = recurrent_branch_rows.shape[0]
    taps = convolution_kernel.shape[0]
    padded = jnp.pad(recurrent_branch_rows.astype(jnp.float32), ((taps - 1, 0), (0, 0)))
    conv_sum = jnp.zeros((length, recurrent_branch_rows.shape[1]), jnp.float32)
    for tap_index in range(taps):
        conv_sum = conv_sum + padded[tap_index : tap_index + length] * convolution_kernel[
            tap_index
        ].astype(jnp.float32)
    conv_rows = conv_sum.astype(jnp.bfloat16)
    blocks = decay_gate_matrix.shape[0]
    blocked = conv_rows.reshape(length, blocks, -1)
    recurrence_gate = jax.nn.sigmoid(
        jnp.einsum(
            "tni,nij->tnj", blocked, decay_gate_matrix, preferred_element_type=jnp.float32
        ).reshape(length, -1)
    )
    input_rate = jax.nn.sigmoid(
        jnp.einsum(
            "tni,nij->tnj", blocked, input_gate_matrix, preferred_element_type=jnp.float32
        ).reshape(length, -1)
    )
    decay_log_values = (
        -8.0 * jax.nn.softplus(-base_decay_logit) * recurrence_gate + extra_log_decay[:, None]
    )
    decay = jnp.exp(decay_log_values)
    drive = (
        jnp.sqrt(-jnp.expm1(2.0 * decay_log_values)) * input_rate * conv_rows.astype(jnp.float32)
    )
    _, hidden = lax.associative_scan(combine, (decay, drive), axis=0)
    return (hidden * gate_branch_rows.astype(jnp.float32)).astype(jnp.bfloat16)


def per_device(
    tokens,
    recurrent_norm_gain,
    feedforward_norm_gain,
    gate_projection_weight,
    recurrent_projection_weight,
    convolution_kernel,
    decay_gate_matrix,
    input_gate_matrix,
    base_decay_logit,
    extra_log_decay,
    output_projection_weight,
    up_projection_weight,
    down_projection_weight,
):
    whole_rows = collect(tokens, "tp", 1)
    normed = rms_rows(whole_rows, recurrent_norm_gain)
    gate_whole, recur_whole, out_whole, up_whole, down_whole = gather_turned(
        (
            gate_projection_weight,
            recurrent_projection_weight,
            output_projection_weight,
            up_projection_weight,
            down_projection_weight,
        ),
        "fs",
        (0, 0, 1, 0, 1),
    )
    gate_pre = jnp.dot(normed, gate_whole, preferred_element_type=jnp.float32)
    recur_pre = jnp.dot(normed, recur_whole, preferred_element_type=jnp.float32)
    gate_branch_rows = jax.nn.gelu(gate_pre).astype(jnp.bfloat16)
    recurrent_branch_rows = recur_pre.astype(jnp.bfloat16)
    mixed_output = recurrent_state(
        recurrent_branch_rows,
        gate_branch_rows,
        convolution_kernel,
        decay_gate_matrix,
        input_gate_matrix,
        base_decay_logit,
        extra_log_decay,
    )
    partials = jnp.dot(mixed_output, out_whole, preferred_element_type=jnp.float32)
    residual = (
        tokens.astype(jnp.float32) + sent_and_summed(partials.astype(jnp.bfloat16), "tp", 1)
    ).astype(jnp.bfloat16)
    middle = collect(residual, "tp", 1)
    channel_in = rms_rows(middle, feedforward_norm_gain)
    upward = jnp.dot(channel_in, up_whole, preferred_element_type=jnp.float32)
    positive = jnp.maximum(upward, 0.0)
    squared = (positive * positive).astype(jnp.bfloat16)
    down_terms = jnp.dot(squared, down_whole, preferred_element_type=jnp.float32)
    summed_down = sent_and_summed(down_terms.astype(jnp.bfloat16), "tp", 1)
    return (residual.astype(jnp.float32) + summed_down).astype(jnp.bfloat16)


def solution(mesh):
    placed = (
        P(("grp", "fs"), "tp"),
        P(),
        P(),
        P("fs", "tp"),
        P("fs", "tp"),
        P(None, "tp"),
        P("tp", None, None),
        P("tp", None, None),
        P("tp"),
        P(("grp", "fs")),
        P("tp", "fs"),
        P("fs", "tp"),
        P("tp", "fs"),
    )
    return jax.shard_map(
        per_device, mesh=mesh, in_specs=placed, out_specs=P(("grp", "fs"), "tp"), check_vma=False
    )
```

profile of v0, /device:TPU:33, one launch (start us, length us, event | category | flops | bytes accessed | tf_op | source)
XLA Modules:
  0.0 277.3 jit_solution(16878927813386436569)
XLA Ops:
  6.6 0.8 constant_dynamic-update-slice_fusion.2
  7.3 0.8 constant_dynamic-update-slice_fusion.1
  8.1 0.8 bitcast_dynamic-update-slice_fusion.1
  8.9 0.9 constant_dynamic-update-slice_fusion
  9.8 0.0 copy-start.7
  9.8 0.0 copy-start.5
  9.8 0.9 bitcast_dynamic-update-slice_fusion
  10.7 0.7 copy-done.2
  11.5 0.1 all-gather.2.cloned.1.call-update
  11.6 1.0 copy.28
  12.6 0.0 copy-start.3
  12.6 1.1 broadcast_in_dim.4
  13.6 44.9 %all-to-all-start = ((bf16[8,256,256]{1,2,0:T(8,128)(2,1)}), bf16[8,256,256]{1,2,0:T(8,128)(2,1)S(1)}, u32[]{:S(2)}, u32[]{:S(2)}) async-start(bf16[8,256,256]{1,2,0:T(8,128)(2,1)} %broadcast_in_dim.4), calls=%async_computation | async-start | bytes 2097152 | tf_op jit(solution)/shard_map/all_to_all | solution.py:9
  58.6 15.0 %all-to-all-done = bf16[8,256,256]{1,2,0:T(8,128)(2,1)S(1)} async-done(((bf16[8,256,256]{1,2,0:T(8,128)(2,1)}), bf16[8,256,256]{1,2,0:T(8,128)(2,1)S(1)}, u32[]{:S(2)}, u32[]{:S(2)}) %all-to-all-start) | async-done | bytes 1048608 | tf_op jit(solution)/shard_map/all_to_all | solution.py:9
  73.6 0.3 multiply_reduce_fusion.1
  73.9 0.3 fusion.10
  74.3 0.0 copy-start.8
  74.3 112.4 %all-gather.2.cloned.1.call-done = bf16[2048,2816]{1,0:T(8,128)(2,1)} async-done(((bf16[64,2816]{1,0:T(8,128)(2,1)}), bf16[2048,2816]{1,0:T(8,128)(2,1)}) %all-gather.2.cloned.1.call-update) | async-done | bytes 11534352 | tf_op jit(solution)/shard_map/all_gather | solution.py:27
  186.7 1.7 fusion.28
  188.4 0.0 copy-start.6
  188.4 0.1 fusion.96
  188.6 0.3 fusion.24
  188.8 0.1 copy.41
  189.0 0.3 fusion.27
  189.3 0.1 copy.40
  189.4 0.3 fusion.59
  189.8 0.1 slice.218
  189.9 0.1 slice.214
  190.0 0.2 slice.213
  190.2 0.2 slice.270
  190.5 0.1 slice.216
  190.6 0.1 slice.215
  192.3 2.9 %convolution_convert_fusion = bf16[256,2048]{1,0:T(8,128)(2,1)S(1)} fusion(bf16[2048,2816]{1,0:T(8,128)(2,1)} %all-gather.2.cloned.1.call-done, bf16[256,2048]{0,1:T(8,128)(2,1)S(1)} %fusion.10, f32[256,256]{1,0:T(8,128)S(1)} %pad.68, f32[256,256]{1,0:T(8,128)S(1)} %pad.69), kind=kOutput, calls=%fused_computation.5 | convolution fusion | flops 538247168 | bytes 4718592 | tf_op jit(solution)/shard_map/dot_general | solution.py:141
  195.2 0.1 copy.56
  195.3 0.0 copy-start.1
  195.3 30.4 %all_to_all.20 = bf16[8,256,256]{2,1,0:T(8,128)(2,1)S(1)} all-to-all(bf16[8,256,256]{2,1,0:T(8,128)(2,1)S(1)} %bitcast.56), channel_id=1, replica_groups=mesh['grp'=2,'fs'=32,'tp'=8] {'tp'}, dimensions={0} | all-to-all | bytes 2097152 | tf_op jit(solution)/shard_map/all_to_all | solution.py:45
  225.7 0.1 convert_reduce_fusion.1
  225.8 0.1 copy.36
  226.0 0.0 copy-start.4
  226.0 0.1 broadcast_in_dim.5
  226.0 18.5 %all_to_all.21 = bf16[8,256,256]{1,2,0:T(8,128)(2,1)S(1)} all-to-all(bf16[8,256,256]{1,2,0:T(8,128)(2,1)S(1)} %broadcast_in_dim.5), channel_id=1, replica_groups=mesh['grp'=2,'fs'=32,'tp'=8] {'tp'}, dimensions={0} | all-to-all | bytes 2097152 | tf_op jit(solution)/shard_map/all_to_all | solution.py:9
  244.5 0.3 multiply_reduce_fusion
  244.8 0.3 fusion.8
  245.2 5.8 %fusion.4 = bf16[256,2048]{1,0:T(8,128)(2,1)S(1)} fusion(bf16[2048,2816]{1,0:T(8,128)(2,1)} %all-gather.2.cloned.1.call-done, bf16[256,2048]{0,1:T(8,128)(2,1)S(1)} %fusion.8), kind=kOutput, calls=%fused_computation.4 | convolution fusion | flops 2148794368 | bytes 10485760 | tf_op jit(solution)/shard_map/dot_general | solution.py:150
  251.0 0.1 copy.55
  251.1 18.5 %all_to_all.22 = bf16[8,256,256]{2,1,0:T(8,128)(2,1)S(1)} all-to-all(bf16[8,256,256]{2,1,0:T(8,128)(2,1)S(1)} %bitcast.57), channel_id=1, replica_groups=mesh['grp'=2,'fs'=32,'tp'=8] {'tp'}, dimensions={0} | all-to-all | bytes 2097152 | tf_op jit(solution)/shard_map/all_to_all | solution.py:45
  269.6 0.1 convert_reduce_fusion
  269.7 0.7 add_convert_fusion
  (99 shorter events, 1.3 us)
Async XLA Ops:
  6.5 182.0 %copy-start = (bf16[2,128,128]{2,1,0:T(8,128)(2,1)S(1)}, bf16[2,128,128]{2,1,0:T(8,128)(2,1)}, u32[]{:S(2)}) copy-start(bf16[2,128,128]{2,1,0:T(8,128)(2,1)} %param.20) | copy-start | bytes 196612
  6.6 180.2 %all-gather.2.cloned.1.call-start = ((), (), s32[]{:S(2)}) async-start(), calls=%async_computation.4 | async-start | bytes 11894784 | tf_op jit(solution)/shard_map/all_gather | solution.py:27
  9.8 48.8 %copy-start.7 = (f32[256]{0:T(256)S(1)}, f32[256]{0:T(256)}, u32[]{:S(2)}) copy-start(f32[256]{0:T(256)} %param.21) | copy-start | bytes 3076
  9.8 48.8 %copy-start.5 = (bf16[4,256]{1,0:T(4,128)(2,1)S(1)}, bf16[4,256]{1,0:T(4,128)(2,1)}, u32[]{:S(2)}) copy-start(bf16[4,256]{1,0:T(4,128)(2,1)} %param.18) | copy-start | bytes 6148
  10.7 0.8 copy-start.2
  12.6 61.4 %copy-start.3 = (f32[2048]{0:T(1024)S(1)}, f32[2048]{0:T(1024)}, u32[]{:S(2)}) copy-start(f32[2048]{0:T(1024)} %param.14) | copy-start | bytes 24580
  13.6 60.0 %all-to-all-start = ((bf16[8,256,256]{1,2,0:T(8,128)(2,1)}), bf16[8,256,256]{1,2,0:T(8,128)(2,1)S(1)}, u32[]{:S(2)}, u32[]{:S(2)}) async-start(bf16[8,256,256]{1,2,0:T(8,128)(2,1)} %broadcast_in_dim.4), calls=%async_computation | async-start | bytes 2097152 | tf_op jit(solution)/shard_map/all_to_all | solution.py:9
  74.3 114.7 %copy-start.8 = (bf16[2,128,128]{2,1,0:T(8,128)(2,1)S(1)}, bf16[2,128,128]{2,1,0:T(8,128)(2,1)}, u32[]{:S(2)}) copy-start(bf16[2,128,128]{2,1,0:T(8,128)(2,1)} %param.19) | copy-start | bytes 196612
  188.4 1.0 copy-start.6
  195.3 30.5 %copy-start.1 = (bf16[256,256]{1,0:T(8,128)(2,1)S(1)}, bf16[256,256]{1,0:T(8,128)(2,1)}, u32[]{:S(2)}) copy-start(bf16[256,256]{1,0:T(8,128)(2,1)} %param.13) | copy-start | bytes 393220
  226.0 18.9 %copy-start.4 = (f32[2048]{0:T(1024)S(1)}, f32[2048]{0:T(1024)}, u32[]{:S(2)}) copy-start(f32[2048]{0:T(1024)} %param.15) | copy-start | bytes 24580
Sparse Core Ops, SparseCore 0:
  11.7 174.9 all-gather.1
where the time goes:
time: 278 us; the launch traced here: 277 us
  waiting for transfers between devices  128 us (46%)
  blocking collectives  67.3 us (24%)
  starting transfers between devices  44.9 us (16%)
  between operations  14.1 us (5%)
  matrix products  11 us (4%)
  local copies, waits for them, and re-layouts  9.37 us (3%)
  other arithmetic  3.14 us (1%)
    all_gather x1, waiting for transfers between devices, gather_turned(): out = lax.all_gather(both, axis, axis=0, tiled=True)  112 us
    all_to_all x2, blocking collectives, sent_and_summed(): tiles = lax.all_to_all(in_blocks(x, dim, peers), axis, 0, 0, tiled=True)  48.8 us
    all_to_all x1, starting transfers between devices, from_everyone(): return lax.all_to_all(copies, axis, split_axis=0, concat_axis=0, tiled=True)  44.9 us
    all_to_all x1, blocking collectives, from_everyone(): return lax.all_to_all(copies, axis, split_axis=0, concat_axis=0, tiled=True)  18.5 us
    all_to_all x1, waiting for transfers between devices, from_everyone(): return lax.all_to_all(copies, axis, split_axis=0, concat_axis=0, tiled=True)  15 us
    dot_general x1, matrix products, per_device(): jnp.dot(squared, down_whole, preferred_element_type=jnp.float32)  5.84 us
  transfers between devices with their start and end apart: 2, of which 2 were waited for; matrix products, arithmetic and copies ran while one was open for 1% of the time, Pallas kernels for 0%

commit v1 on v0

--- a/solution.py
+++ b/solution.py
@@ -24,7 +24,9 @@
     turned = [jnp.moveaxis(a, dim, 0) for a, dim in zip(arrays, dims)]
     widths = [t[0].size for t in turned]
     both = jnp.concatenate([t.reshape(-1, w) for t, w in zip(turned, widths)], axis=1)
-    out = lax.all_gather(both, axis, axis=0, tiled=True)
+    out = jnp.concatenate(
+        lax.all_to_all(jnp.stack([both] * lax.axis_size(axis)), axis, 0, 0), axis=0
+    )
     tiles = jnp.split(out, [sum(widths[:k]) for k in range(1, len(widths))], axis=1)
     return tuple(
         (

time: 278 us -> 1150 us (4.14)
  the two profiles are of different devices: /device:TPU:33 before, /device:TPU:232 now
where the time goes in v1:
time: 1150 us
  waiting for transfers between devices  1020 us (89%)
  blocking collectives  55.6 us (5%)
  starting transfers between devices  46.4 us (4%)
    all_to_all x1, waiting for transfers between devices, gather_turned(): lax.all_to_all(jnp.stack([both] * lax.axis_size(axis)), axis, 0, 0)  1010 us
    all_to_all x1, starting transfers between devices, gather_turned(): lax.all_to_all(jnp.stack([both] * lax.axis_size(axis)), axis, 0, 0)  41.8 us
    all_to_all x2, blocking collectives, sent_and_summed(): tiles = lax.all_to_all(in_blocks(x, dim, peers), axis, 0, 0, tiled=True)  37.1 us
  transfers between devices with their start and end apart: 2, of which 2 were waited for; matrix products, arithmetic and copies ran while one was open for 0% of the time, Pallas kernels for 0%

profile of v1, /device:TPU:232, one launch (start us, length us, event | category | flops | bytes accessed | tf_op | source)
XLA Modules:
  0.0 1147.9 jit_solution(8582600106492224976)
XLA Ops:
  0.0 0.0 copy-start
  0.0 0.0 copy-start.6
  0.0 0.0 copy-start.2
  0.0 0.0 copy-start.3
  0.0 1.1 copy.28
  1.1 1.0 broadcast_in_dim.4
  2.2 4.6 all-to-all-start
  6.7 0.0 copy-done.4
  6.8 0.0 copy-done.5
  6.9 15.8 %all-to-all-done = bf16[8,256,256]{1,2,0:T(8,128)(2,1)S(1)} async-done(((bf16[8,256,256]{1,2,0:T(8,128)(2,1)}), bf16[8,256,256]{1,2,0:T(8,128)(2,1)S(1)}, u32[]{:S(2)}, u32[]{:S(2)}) %all-to-all-start) | async-done | bytes 1048608 | tf_op jit(solution)/shard_map/all_to_all | solution.py:9
  22.7 5.5 stack.2
  28.2 41.8 %all-to-all-start.1 = ((bf16[32,64,2816]{2,1,0:T(8,128)(2,1)}), bf16[32,64,2816]{2,1,0:T(8,128)(2,1)}, u32[]{:S(2)}, u32[]{:S(2)}) async-start(bf16[32,64,2816]{2,1,0:T(8,128)(2,1)} %stack.2), calls=%async_computation.1 | async-start | bytes 23068672 | tf_op jit(solution)/shard_map/all_to_all | solution.py:28
  70.1 0.0 copy-done.11
  70.1 0.3 multiply_reduce_fusion.1
  70.4 0.3 fusion.10
  70.8 1005.2 %all-to-all-done.1 = bf16[32,64,2816]{2,1,0:T(8,128)(2,1)} async-done(((bf16[32,64,2816]{2,1,0:T(8,128)(2,1)}), bf16[32,64,2816]{2,1,0:T(8,128)(2,1)}, u32[]{:S(2)}, u32[]{:S(2)}) %all-to-all-start.1) | async-done | bytes 11534368 | tf_op jit(solution)/shard_map/all_to_all | solution.py:28
  1075.9 1.7 fusion.28
  1077.7 0.0 copy-start.10
  1077.7 0.1 fusion.96
  1077.8 0.3 fusion.27
  1078.1 0.1 copy.40
  1078.2 0.0 copy-done.12
  1078.2 0.3 fusion.24
  1078.5 0.1 copy.41
  1078.7 0.3 fusion.59
  1079.0 0.2 slice.213
  1079.3 0.1 slice.218
  1079.4 0.1 slice.214
  1079.5 0.2 slice.270
  1079.7 0.1 slice.216
  1079.8 0.1 slice.215
  1081.6 2.9 convolution_convert_fusion
  1084.5 0.1 copy.56
  1084.5 0.0 copy-start.1
  1084.6 18.6 %all_to_all.25 = bf16[8,256,256]{2,1,0:T(8,128)(2,1)S(1)} all-to-all(bf16[8,256,256]{2,1,0:T(8,128)(2,1)S(1)} %bitcast.57), channel_id=1, replica_groups=mesh['grp'=2,'fs'=32,'tp'=8] {'tp'}, dimensions={0} | all-to-all | bytes 2097152 | tf_op jit(solution)/shard_map/all_to_all | solution.py:47
  1103.2 0.1 convert_reduce_fusion.1
  1103.3 0.0 copy-done.1
  1103.4 0.1 copy.36
  1103.5 0.0 copy-start.8
  1103.5 0.1 broadcast_in_dim.5
  1103.6 18.5 %all_to_all.26 = bf16[8,256,256]{1,2,0:T(8,128)(2,1)S(1)} all-to-all(bf16[8,256,256]{1,2,0:T(8,128)(2,1)S(1)} %broadcast_in_dim.5), channel_id=1, replica_groups=mesh['grp'=2,'fs'=32,'tp'=8] {'tp'}, dimensions={0} | all-to-all | bytes 2097152 | tf_op jit(solution)/shard_map/all_to_all | solution.py:9
  1122.0 0.3 multiply_reduce_fusion
  1122.3 0.3 fusion.8
  1122.7 5.8 fusion.4
  1128.5 0.1 copy.55
  1128.6 18.5 %all_to_all.27 = bf16[8,256,256]{2,1,0:T(8,128)(2,1)S(1)} all-to-all(bf16[8,256,256]{2,1,0:T(8,128)(2,1)S(1)} %bitcast.58), channel_id=1, replica_groups=mesh['grp'=2,'fs'=32,'tp'=8] {'tp'}, dimensions={0} | all-to-all | bytes 2097152 | tf_op jit(solution)/shard_map/all_to_all | solution.py:47
  1147.1 0.1 convert_reduce_fusion
  1147.2 0.7 add_convert_fusion
  (107 shorter events, 1.4 us)
Async XLA Ops:
  0.0 1077.8 %copy-start = (bf16[2,128,128]{2,1,0:T(8,128)(2,1)S(1)}, bf16[2,128,128]{2,1,0:T(8,128)(2,1)}, u32[]{:S(2)}) copy-start(bf16[2,128,128]{2,1,0:T(8,128)(2,1)} %param.19) | copy-start | bytes 196612
  0.0 6.7 copy-start.4
  0.0 6.8 copy-start.5
  0.0 6.8 copy-start.6
  0.0 6.8 copy-start.2
  0.0 6.8 copy-start.3
  2.2 20.5 %all-to-all-start = ((bf16[8,256,256]{1,2,0:T(8,128)(2,1)}), bf16[8,256,256]{1,2,0:T(8,128)(2,1)S(1)}, u32[]{:S(2)}, u32[]{:S(2)}) async-start(bf16[8,256,256]{1,2,0:T(8,128)(2,1)} %broadcast_in_dim.4), calls=%async_computation | async-start | bytes 2097152 | tf_op jit(solution)/shard_map/all_to_all | solution.py:9
  28.2 41.8 %copy-start.11 = (f32[256]{0:T(256)S(1)}, f32[256]{0:T(256)}, u32[]{:S(2)}) copy-start(f32[256]{0:T(256)} %param.21) | copy-start | bytes 3076
  28.2 41.9 %copy-start.9 = (bf16[4,256]{1,0:T(4,128)(2,1)S(1)}, bf16[4,256]{1,0:T(4,128)(2,1)}, u32[]{:S(2)}) copy-start(bf16[4,256]{1,0:T(4,128)(2,1)} %param.18) | copy-start | bytes 6148
  28.2 42.2 %copy-start.7 = (f32[2048]{0:T(1024)S(1)}, f32[2048]{0:T(1024)}, u32[]{:S(2)}) copy-start(f32[2048]{0:T(1024)} %param.14) | copy-start | bytes 24580
  28.2 1047.7 %all-to-all-start.1 = ((bf16[32,64,2816]{2,1,0:T(8,128)(2,1)}), bf16[32,64,2816]{2,1,0:T(8,128)(2,1)}, u32[]{:S(2)}, u32[]{:S(2)}) async-start(bf16[32,64,2816]{2,1,0:T(8,128)(2,1)} %stack.2), calls=%async_computation.1 | async-start | bytes 23068672 | tf_op jit(solution)/shard_map/all_to_all | solution.py:28
  1075.9 2.3 copy-start.12
  1077.7 1.0 copy-start.10
  1084.5 18.8 %copy-start.1 = (bf16[256,256]{1,0:T(8,128)(2,1)S(1)}, bf16[256,256]{1,0:T(8,128)(2,1)}, u32[]{:S(2)}) copy-start(bf16[256,256]{1,0:T(8,128)(2,1)} %param.13) | copy-start | bytes 393220
  1103.5 18.9 %copy-start.8 = (f32[2048]{0:T(1024)S(1)}, f32[2048]{0:T(1024)}, u32[]{:S(2)}) copy-start(f32[2048]{0:T(1024)} %param.15) | copy-start | bytes 24580
